TPU v7x, 32 devices: a whole 2x2x4 slice. The times are simulated.
32 devices in a mesh: grp: 2 (over y), ep: 8 (over z, x), tp: 2 (over core).
Axes of the slice: x: 2, y: 2, z: 4, core: 2. Of those that a mesh axis runs over, the one named last changes fastest.
Arguments:
- tokens: bfloat16 [512, 2048], P(('grp', 'ep'), 'tp'), parts along dimension 0, may hold values from -6 to 6
- gain: float32 [2048], replicated, may hold values from 0.1 to 1.9
- routes: int32 [512, 4], P(('grp', 'ep')), parts along dimension 0, may hold values from 0 to 7, all different within a row; in each aligned block of 32 rows (0 to 31, 32 to 63, ...) at most 32 rows name the same one
- weights: float32 [512, 4], P(('grp', 'ep')), parts along dimension 0, may hold values from 0.05 to 1
- w_gate: bfloat16 [8, 2048, 6144], P('ep', None, 'tp'), may hold values from -0.125 to 0.125
- w_up: bfloat16 [8, 2048, 6144], P('ep', None, 'tp'), may hold values from -0.125 to 0.125
- w_down: bfloat16 [8, 6144, 2048], P('ep', 'tp'), may hold values from -0.078125 to 0.078125
Outputs:
- mixed: bfloat16 [512, 2048], P(('grp', 'ep'), 'tp'), parts along dimension 0
There are 2 independent parts, one for each index of `grp`. A program takes and returns all parts, laid end to end along the dimension named above; an argument that names none is the same for every part. Nothing has to cross between parts.
Inputs may be any that keep to these rules, and one draw needn't show every extreme that they name: `routes`: each row names 4 different experts. Among the rows of one device no expert is named by more than 32 rows, a bound that some block reaches.
All inputs are finite; a program needn't handle non-finite values.
Results may differ from a plain program's by a relative error of at most 0.019.
Values may be sent and summed in bfloat16 or wider, within the bound.
No kernel may reach another device: no remote copies, remote signals or barrier semaphores. Data moves between devices by JAX's collectives and lax.ppermute only.
A program may use at most 128 MiB of HBM per device.

v0:
```python
import jax
import jax.numpy as jnp
from jax import lax
from jax.sharding import PartitionSpec as P

epsilon = 1e-05


def expert_rows(chosen, gate_w, up_w, down_w):
    gate_val = jnp.dot(chosen, gate_w, preferred_element_type=jnp.float32)
    up_val = jnp.dot(chosen, up_w, preferred_element_type=jnp.float32)
    hidden = (jax.nn.silu(gate_val) * up_val).astype(jnp.bfloat16)
    partial_value = jnp.dot(hidden, down_w, preferred_element_type=jnp.float32).astype(jnp.bfloat16)
    return (
        lax.psum_scatter(partial_value, "tp", scatter_dimension=1, tiled=True)
        .astype(jnp.float32)
        .astype(jnp.bfloat16)
    )


def on_device(tokens, gain, routes, weights, w_gate, w_up, w_down):
    groups = lax.axis_size("ep")
    shards = lax.axis_size("tp")
    tok_rows, top_count = routes.shape
    capacity = min(tok_rows, 2 * tok_rows * top_count // groups)
    gate_w, up_w, down_w = (w_gate[0], w_up[0], w_down[0])
    values = tokens.astype(jnp.float32)
    own_width = values.shape[1]
    width = own_width * shards
    totals = lax.psum((jnp.sum(values, axis=1), jnp.sum(values * values, axis=1)), "tp")
    average = totals[0] / width
    spread = totals[1] / width - average * average
    local_gain = lax.dynamic_slice_in_dim(gain, lax.axis_index("tp") * own_width, own_width)
    normed = (
        (values - average[:, None]) * lax.rsqrt(spread[:, None] + epsilon) * local_gain
    ).astype(jnp.bfloat16)
    pair_expert = routes.reshape(-1)
    pair_token = jnp.arange(tok_rows * top_count, dtype=jnp.int32) // top_count
    member = (pair_expert[:, None] == jnp.arange(groups, dtype=jnp.int32)[None, :]).astype(
        jnp.int32
    )
    earlier = jnp.cumsum(member, axis=0) - member
    position = pair_expert * capacity + jnp.sum(earlier * member, axis=1)
    row_width = normed.shape[1]
    outbox = (
        jnp.zeros((groups * capacity, row_width), jnp.bfloat16).at[position].set(normed[pair_token])
    )
    outbox = outbox.reshape(groups, capacity, row_width)
    arrived = lax.all_gather(
        lax.all_to_all(outbox, "ep", split_axis=0, concat_axis=0, tiled=True),
        "tp",
        axis=2,
        tiled=True,
    )
    count = arrived.shape[1]
    flat_rows = arrived.reshape(groups * count, arrived.shape[2])
    served = expert_rows(flat_rows, gate_w, up_w, down_w).reshape(groups, count, -1)
    returned = lax.all_to_all(served, "ep", split_axis=0, concat_axis=0, tiled=True)
    picked = (
        returned.reshape(groups * capacity, -1)[position]
        .reshape(tok_rows, top_count, -1)
        .astype(jnp.float32)
    )
    return jnp.sum(picked * weights[:, :, None], axis=1).astype(jnp.bfloat16)


def solution(mesh):
    in_specs = (
        P(("grp", "ep"), "tp"),
        P(),
        P(("grp", "ep"), None),
        P(("grp", "ep"), None),
        P("ep", None, "tp"),
        P("ep", None, "tp"),
        P("ep", "tp", None),
    )
    out_specs = P(("grp", "ep"), "tp")
    return jax.shard_map(
        on_device, mesh=mesh, in_specs=in_specs, out_specs=out_specs, check_vma=False
    )
```

profile of v0, /device:TPU:0, one launch (start us, length us, event | category | flops | bytes accessed | tf_op | source)
XLA Modules:
  0.0 112.8 jit_solution(12843658255355050022)
XLA Ops:
  6.5 0.0 all-gather.2.cloned.1.call-start
  6.5 0.8 copy.12
  7.3 0.7 broadcast_multiply_fusion
  8.0 1.0 convert_reduce_fusion
  9.0 0.1 eq.15
  9.1 0.1 fusion.24
  9.2 0.2 reduce_window_sum.11
  9.3 0.2 select_reduce_fusion
  9.5 0.1 copy.11
  9.6 0.1 mul.57
  9.7 2.6 %all-reduce = (f32[32]{0:T(128)S(1)}, f32[32]{0:T(128)S(1)}) all-reduce(f32[32]{0:T(128)S(1)} %get-tuple-element.6, f32[32]{0:T(128)S(1)} %get-tuple-element.5), channel_id=1, replica_groups=mesh['grp'=2,'ep'=8,'tp'=2] {'tp'}, use_global_device_ids=true, to_apply=%region_5.6 | all-reduce | flops 64 | bytes 512 | tf_op jit(solution)/shard_map/psum | solution.py:30
  12.4 0.7 dynamic_slice.3
  13.1 0.9 fusion.22
  14.0 2.2 %scatter_custom_fusion = bf16[256,1024]{1,0:T(8,128)(2,1)S(1)} fusion(s32[128]{0:T(128)S(1)} %fusion.26, bf16[32,1024]{1,0:T(8,128)(2,1)S(1)} %fusion.22, s32[1024]{0:T(1024)S(1)} %pad_clamp_fusion.1, bf16[]{:T(256)} %constant.34.clone.1), kind=kCustom, calls=%fused_computation.13 | custom fusion | bytes 524290 | tf_op jit(solution)/shard_map/scatter | solution.py:46
  16.2 21.8 %all_to_all.10 = bf16[8,32,1024]{2,1,0:T(8,128)(2,1)} all-to-all(bf16[8,32,1024]{2,1,0:T(8,128)(2,1)S(1)} %bitcast.32), channel_id=1, replica_groups=mesh['grp'=2,'ep'=8,'tp'=2] {'ep'}, dimensions={0} | all-to-all | bytes 1048576 | tf_op jit(solution)/shard_map/all_to_all | solution.py:50
  38.0 0.0 all-gather.2.cloned.1.call-update
  38.1 0.0 reduce-scatter.2.cloned.1.call-start
  38.1 8.2 %all-gather.2.cloned.1.call-done = bf16[8,32,2048]{2,1,0:T(8,128)(2,1)} async-done(((bf16[8,32,1024]{2,1,0:T(8,128)(2,1)}), bf16[8,32,2048]{2,1,0:T(8,128)(2,1)}) %all-gather.2.cloned.1.call-update) | async-done | bytes 1048592 | tf_op jit(solution)/shard_map/all_gather | solution.py:49
  46.3 0.0 copy-start.1
  46.3 10.1 %fusion.4 = f32[256,3072]{1,0:T(8,128)} fusion(bf16[256,2048]{1,0:T(8,128)(2,1)} %bitcast.34, bf16[1,2048,3072]{2,1,0:T(8,128)(2,1)} %param.11), kind=kOutput, calls=%fused_computation.7 | convolution fusion | flops 3221225472 | bytes 16777216 | tf_op jit(solution)/shard_map/dot_general | solution.py:10
  56.4 0.0 copy-done.1
  56.4 0.0 copy-start
  56.4 17.0 %fusion.12 = bf16[256,2048]{1,0:T(8,128)(2,1)} fusion(bf16[1,3072,2048]{2,1,0:T(8,128)(2,1)} %param.13, bf16[256,2048]{1,0:T(8,128)(2,1)S(1)} %bitcast.35, bf16[1,2048,3072]{2,1,0:T(8,128)(2,1)} %param.12, f32[256,3072]{1,0:T(8,128)} %fusion.4), kind=kOutput, calls=%fused_computation.11 | convolution fusion | flops 6447693824 | bytes 30408704 | tf_op jit(solution)/shard_map/dot_general | solution.py:13
  73.4 0.0 reduce-scatter.2.cloned.1.call-update
  73.5 9.7 %reduce-scatter.2.cloned.1.call-done = bf16[256,1024]{1,0:T(8,128)(2,1)} async-done(((bf16[256,2048]{1,0:T(8,128)(2,1)}), bf16[256,1024]{1,0:T(8,128)(2,1)}) %reduce-scatter.2.cloned.1.call-update) | async-done | bytes 524304 | tf_op jit(solution)/shard_map/reduce_scatter | solution.py:15
  83.2 5.8 %all-to-all-start.1 = ((bf16[8,32,1024]{2,1,0:T(8,128)(2,1)}), bf16[8,32,1024]{2,1,0:T(8,128)(2,1)S(1)}, u32[]{:S(2)}, u32[]{:S(2)}) async-start(bf16[8,32,1024]{2,1,0:T(8,128)(2,1)} %bitcast.33), calls=%async_computation.2 | async-start | bytes 1048576 | tf_op jit(solution)/shard_map/all_to_all | solution.py:58
  88.9 0.0 copy-done
  88.9 0.1 copy.13
  89.0 14.8 %all-to-all-done.1 = bf16[8,32,1024]{2,1,0:T(8,128)(2,1)S(1)} async-done(((bf16[8,32,1024]{2,1,0:T(8,128)(2,1)}), bf16[8,32,1024]{2,1,0:T(8,128)(2,1)S(1)}, u32[]{:S(2)}, u32[]{:S(2)}) %all-to-all-start.1) | async-done | bytes 524320 | tf_op jit(solution)/shard_map/all_to_all | solution.py:58
  103.9 0.9 gather_fusion
  104.7 0.2 reshape.98
  104.9 1.0 multiply_reduce_fusion
  (5 shorter events, 0.0 us)
Async XLA Ops:
  6.5 39.8 %all-gather.2.cloned.1.call-start = ((), (), s32[]{:S(2)}) async-start(), calls=%async_computation.3 | async-start | bytes 1572864 | tf_op jit(solution)/shard_map/all_gather | solution.py:49
  38.1 45.1 %reduce-scatter.2.cloned.1.call-start = ((), (), s32[]{:S(2)}) async-start(), calls=%async_computation.4 | async-start | bytes 1572864 | tf_op jit(solution)/shard_map/reduce_scatter | solution.py:15
  46.3 10.1 %copy-start.1 = (bf16[8,32,2048]{2,1,0:T(8,128)(2,1)S(1)}, bf16[8,32,2048]{2,1,0:T(8,128)(2,1)}, u32[]{:S(2)}) copy-start(bf16[8,32,2048]{2,1,0:T(8,128)(2,1)} %all-gather.2.cloned.1.call-done) | copy-start | bytes 3145732
  56.4 32.5 %copy-start = (f32[32,4]{0,1:T(4,128)S(1)}, f32[32,4]{0,1:T(4,128)}, u32[]{:S(2)}) copy-start(f32[32,4]{0,1:T(4,128)} %param.10) | copy-start | bytes 1540
  83.2 20.7 %all-to-all-start.1 = ((bf16[8,32,1024]{2,1,0:T(8,128)(2,1)}), bf16[8,32,1024]{2,1,0:T(8,128)(2,1)S(1)}, u32[]{:S(2)}, u32[]{:S(2)}) async-start(bf16[8,32,1024]{2,1,0:T(8,128)(2,1)} %bitcast.33), calls=%async_computation.2 | async-start | bytes 1048576 | tf_op jit(solution)/shard_map/all_to_all | solution.py:58
Sparse Core Ops, SparseCore 0:
  38.2 8.0 all-gather.1
  73.6 9.5 reduce-scatter.1
where the time goes:
time: 113 us
  waiting for transfers between devices  32.8 us (29%)
  matrix products  27.1 us (24%)
  blocking collectives  24.5 us (22%)
  between operations  13.5 us (12%)
  starting transfers between devices  5.82 us (5%)
  local copies, waits for them, and re-layouts  5.08 us (4%)
  other arithmetic  4.06 us (4%)
    all_to_all x1, blocking collectives, on_device(): lax.all_to_all(outbox, 'ep', split_axis=0, concat_axis=0, tiled=True)  21.8 us
    dot_general x1, matrix products, expert_rows(): jnp.dot(hidden, down_w, preferred_element_type=jnp.float32)  17 us
    all_to_all x1, waiting for transfers between devices, on_device(): lax.all_to_all(served, 'ep', split_axis=0, concat_axis=0, tiled=True)  14.8 us
    dot_general x1, matrix products, expert_rows(): gate_val = jnp.dot(chosen, gate_w, preferred_element_type=jnp.float32)  10.1 us
    reduce_scatter x1, waiting for transfers between devices, expert_rows(): lax.psum_scatter(partial_value, 'tp', scatter_dimension=1, tiled=True)  9.7 us
    all_gather x1, waiting for transfers between devices, on_device(): lax.all_gather(lax.all_to_all(outbox, 'ep', split_axis=0, concat_axis=0,...  8.21 us
    all_to_all x1, starting transfers between devices, on_device(): lax.all_to_all(served, 'ep', split_axis=0, concat_axis=0, tiled=True)  5.78 us
    psum x1, blocking collectives, on_device(): lax.psum((jnp.sum(values, axis=1), jnp.sum(values * values, axis=1)), 'tp')  2.63 us
  transfers between devices with their start and end apart: 3, of which 3 were waited for; matrix products, arithmetic and copies ran while one was open for 0% of the time, Pallas kernels for 0%

commit v1 on v0

--- a/solution.py
+++ b/solution.py
@@ -4,6 +4,29 @@
 from jax.sharding import PartitionSpec as P
 
 epsilon = 1e-05
+
+
+def in_blocks(x, dim, size):
+    before, after = (x.shape[:dim], x.shape[dim + 1 :])
+    return jnp.moveaxis(x.reshape(*before, size, -1, *after), dim, 0)
+
+
+def in_order(blocks, dim):
+    blocks = jnp.moveaxis(blocks, 0, dim)
+    dims = blocks.shape
+    return blocks.reshape(*dims[:dim], dims[dim] * dims[dim + 1], *dims[dim + 2 :])
+
+
+def sent_to_each(shard, axis, split_dim, concat_dim):
+    peers, here = (lax.axis_size(axis), lax.axis_index(axis))
+    blocks = in_blocks(shard, split_dim, peers)
+    whole = blocks
+    for step in range(1, peers):
+        target, source = ((here + step) % peers, (here - step) % peers)
+        sent = lax.dynamic_index_in_dim(blocks, target, 0)
+        other = lax.ppermute(sent, axis, [(i, (i + step) % peers) for i in range(peers)])
+        whole = lax.dynamic_update_slice_in_dim(whole, other, source, axis=0)
+    return in_order(whole, concat_dim)
 
 
 def expert_rows(chosen, gate_w, up_w, down_w):
@@ -46,12 +69,7 @@
         jnp.zeros((groups * capacity, row_width), jnp.bfloat16).at[position].set(normed[pair_token])
     )
     outbox = outbox.reshape(groups, capacity, row_width)
-    arrived = lax.all_gather(
-        lax.all_to_all(outbox, "ep", split_axis=0, concat_axis=0, tiled=True),
-        "tp",
-        axis=2,
-        tiled=True,
-    )
+    arrived = lax.all_gather(sent_to_each(outbox, "ep", 0, 0), "tp", axis=2, tiled=True)
     count = arrived.shape[1]
     flat_rows = arrived.reshape(groups * count, arrived.shape[2])
     served = expert_rows(flat_rows, gate_w, up_w, down_w).reshape(groups, count, -1)

time: 113 us -> 111 us (0.982)
  blocking collectives: 24.5 us -> 2.6 us
  starting transfers between devices: 5.82 us -> 19.5 us
  waiting for transfers between devices: 32.8 us -> 38.1 us
    all_to_all x1 -> x0, blocking collectives: 21.8 us -> none  [on_device(): lax.all_to_all(outbox, 'ep', split_axis=0, concat_axis=0, tiled=True)]
    ppermute x0 -> x7, starting transfers between devices: none -> 13.7 us  [sent_to_each(): lax.ppermute(sent, axis, [(i, (i + step) % peers) for i in range(peers)])]
    ppermute x0 -> x7, waiting for transfers between devices: none -> 3.39 us  [sent_to_each(): lax.ppermute(sent, axis, [(i, (i + step) % peers) for i in range(peers)])]
    all_gather x1, waiting for transfers between devices: 8.21 us -> 10.1 us  [on_device(): lax.all_gather(sent_to_each(outbox, 'ep', 0, 0), 'tp', axis=2, tiled=True)]
  transfers between devices with their start and end apart: 3 -> 10, of which waited for: 3 -> 7; matrix products, arithmetic and copies ran while one was open for 0% -> 0% of each run, Pallas kernels for 0% -> 0%
where the time goes in v1:
time: 111 us
  waiting for transfers between devices  38.1 us (34%)
  matrix products  27.1 us (24%)
  starting transfers between devices  19.5 us (18%)
  between operations  13.6 us (12%)
  local copies, waits for them, and re-layouts  5.97 us (5%)
  other arithmetic  4.06 us (4%)
  blocking collectives  2.6 us (2%)
    dot_general x1, matrix products, expert_rows(): jnp.dot(hidden, down_w, preferred_element_type=jnp.float32)  17 us
    all_to_all x1, waiting for transfers between devices, on_device(): lax.all_to_all(served, 'ep', split_axis=0, concat_axis=0, tiled=True)  14.9 us
    ppermute x7, starting transfers between devices, sent_to_each(): lax.ppermute(sent, axis, [(i, (i + step) % peers) for i in range(peers)])  13.7 us
    all_gather x1, waiting for transfers between devices, on_device(): lax.all_gather(sent_to_each(outbox, 'ep', 0, 0), 'tp', axis=2, tiled=True)  10.1 us
    dot_general x1, matrix products, expert_rows(): gate_val = jnp.dot(chosen, gate_w, preferred_element_type=jnp.float32)  10.1 us
    reduce_scatter x1, waiting for transfers between devices, expert_rows(): lax.psum_scatter(partial_value, 'tp', scatter_dimension=1, tiled=True)  9.7 us
    all_to_all x1, starting transfers between devices, on_device(): lax.all_to_all(served, 'ep', split_axis=0, concat_axis=0, tiled=True)  5.77 us
    ppermute x7, waiting for transfers between devices, sent_to_each(): lax.ppermute(sent, axis, [(i, (i + step) % peers) for i in range(peers)])  3.39 us
  transfers between devices with their start and end apart: 10, of which 7 were waited for; matrix products, arithmetic and copies ran while one was open for 0% of the time, Pallas kernels for 0%

profile of v1, /device:TPU:0, one launch (start us, length us, event | category | flops | bytes accessed | tf_op | source)
XLA Modules:
  0.0 110.9 jit_solution(15109805350046220212)
XLA Ops:
  6.5 0.0 all-gather.2.cloned.1.call-start
  6.5 0.8 copy.12
  7.3 0.7 broadcast_multiply_fusion
  8.0 1.0 convert_reduce_fusion
  8.9 0.1 eq.30
  9.1 0.1 fusion.24
  9.2 0.2 reduce_window_sum.11
  9.3 0.2 select_reduce_fusion
  9.5 0.1 copy.11
  9.6 0.1 mul.57
  9.8 0.7 dynamic_slice.25
  10.5 2.6 %all-reduce = (f32[32]{0:T(128)S(1)}, f32[32]{0:T(128)S(1)}) all-reduce(f32[32]{0:T(128)S(1)} %get-tuple-element.6, f32[32]{0:T(128)S(1)} %get-tuple-element.5), channel_id=1, replica_groups=mesh['grp'=2,'ep'=8,'tp'=2] {'tp'}, use_global_device_ids=true, to_apply=%region_5.6 | all-reduce | flops 64 | bytes 512 | tf_op jit(solution)/shard_map/psum | solution.py:53
  13.1 0.9 fusion.22
  14.0 2.2 %scatter_custom_fusion = bf16[256,1024]{1,0:T(8,128)(2,1)S(1)} fusion(s32[128]{0:T(128)S(1)} %get-tuple-element.19, bf16[32,1024]{1,0:T(8,128)(2,1)S(1)} %fusion.22, s32[1024]{0:T(1024)S(1)} %pad_clamp_fusion.1, bf16[]{:T(256)} %constant.135.clone.1), kind=kCustom, calls=%fused_computation.13 | custom fusion | bytes 524290 | tf_op jit(solution)/shard_map/scatter | solution.py:69
  16.3 2.9 %collective-permute-start = (bf16[1,1,32,1024]{3,2,0,1:T(8,128)(2,1)S(1)}, bf16[1,1,32,1024]{3,2,0,1:T(8,128)(2,1)S(1)}, u32[]{:S(2)}, u32[]{:S(2)}) collective-permute-start(bf16[1,1,32,1024]{3,2,0,1:T(8,128)(2,1)S(1)} %get-tuple-element.15), channel_id=1, source_target_pairs={{0,2},{2,4},{4,6},{6,8},{8,10},{10,12},{12,14},{14,0},{1,3},{3,5},... | collective-permute-start | bytes 196616 | tf_op jit(solution)/shard_map/ppermute | solution.py:27
  19.1 1.6 %collective-permute-start.1 = (bf16[1,1,32,1024]{3,2,0,1:T(8,128)(2,1)S(1)}, bf16[1,1,32,1024]{3,2,0,1:T(8,128)(2,1)S(1)}, u32[]{:S(2)}, u32[]{:S(2)}) collective-permute-start(bf16[1,1,32,1024]{3,2,0,1:T(8,128)(2,1)S(1)} %get-tuple-element.14), channel_id=1, source_target_pairs={{0,4},{2,6},{4,8},{6,10},{8,12},{10,14},{12,0},{14,2},{1,5},{3,7},... | collective-permute-start | bytes 196616 | tf_op jit(solution)/shard_map/ppermute | solution.py:27
  20.7 2.6 %collective-permute-start.2 = (bf16[1,1,32,1024]{3,2,0,1:T(8,128)(2,1)S(1)}, bf16[1,1,32,1024]{3,2,0,1:T(8,128)(2,1)S(1)}, u32[]{:S(2)}, u32[]{:S(2)}) collective-permute-start(bf16[1,1,32,1024]{3,2,0,1:T(8,128)(2,1)S(1)} %get-tuple-element.13), channel_id=1, source_target_pairs={{0,6},{2,8},{4,10},{6,12},{8,14},{10,0},{12,2},{14,4},{1,7},{3,9},... | collective-permute-start | bytes 196616 | tf_op jit(solution)/shard_map/ppermute | solution.py:27
  23.3 1.2 %collective-permute-start.3 = (bf16[1,1,32,1024]{3,2,0,1:T(8,128)(2,1)S(1)}, bf16[1,1,32,1024]{3,2,0,1:T(8,128)(2,1)S(1)}, u32[]{:S(2)}, u32[]{:S(2)}) collective-permute-start(bf16[1,1,32,1024]{3,2,0,1:T(8,128)(2,1)S(1)} %get-tuple-element.12), channel_id=1, source_target_pairs={{0,8},{2,10},{4,12},{6,14},{8,0},{10,2},{12,4},{14,6},{1,9},{3,11}... | collective-permute-start | bytes 196616 | tf_op jit(solution)/shard_map/ppermute | solution.py:27
  24.5 2.6 %collective-permute-start.4 = (bf16[1,1,32,1024]{3,2,0,1:T(8,128)(2,1)S(1)}, bf16[1,1,32,1024]{3,2,0,1:T(8,128)(2,1)S(1)}, u32[]{:S(2)}, u32[]{:S(2)}) collective-permute-start(bf16[1,1,32,1024]{3,2,0,1:T(8,128)(2,1)S(1)} %get-tuple-element.11), channel_id=1, source_target_pairs={{0,10},{2,12},{4,14},{6,0},{8,2},{10,4},{12,6},{14,8},{1,11},{3,13... | collective-permute-start | bytes 196616 | tf_op jit(solution)/shard_map/ppermute | solution.py:27
  27.1 0.0 collective-permute-done
  27.1 1.3 %collective-permute-start.5 = (bf16[1,1,32,1024]{3,2,0,1:T(8,128)(2,1)S(1)}, bf16[1,1,32,1024]{3,2,0,1:T(8,128)(2,1)S(1)}, u32[]{:S(2)}, u32[]{:S(2)}) collective-permute-start(bf16[1,1,32,1024]{3,2,0,1:T(8,128)(2,1)S(1)} %get-tuple-element.10), channel_id=1, source_target_pairs={{0,12},{2,14},{4,0},{6,2},{8,4},{10,6},{12,8},{14,10},{1,13},{3,15... | collective-permute-start | bytes 196616 | tf_op jit(solution)/shard_map/ppermute | solution.py:27
  28.5 0.0 collective-permute-done.1
  28.5 1.5 %collective-permute-start.6 = (bf16[1,1,32,1024]{3,2,0,1:T(8,128)(2,1)S(1)}, bf16[1,1,32,1024]{3,2,0,1:T(8,128)(2,1)S(1)}, u32[]{:S(2)}, u32[]{:S(2)}) collective-permute-start(bf16[1,1,32,1024]{3,2,0,1:T(8,128)(2,1)S(1)} %get-tuple-element.9), channel_id=1, source_target_pairs={{0,14},{2,0},{4,2},{6,4},{8,6},{10,8},{12,10},{14,12},{1,15},{3,1}... | collective-permute-start | bytes 196616 | tf_op jit(solution)/shard_map/ppermute | solution.py:27
  30.0 0.5 collective-permute-done.2
  30.5 0.8 collective-permute-done.3
  31.4 0.9 collective-permute-done.4
  32.3 1.1 %collective-permute-done.5 = bf16[1,1,32,1024]{3,2,0,1:T(8,128)(2,1)S(1)} collective-permute-done((bf16[1,1,32,1024]{3,2,0,1:T(8,128)(2,1)S(1)}, bf16[1,1,32,1024]{3,2,0,1:T(8,128)(2,1)S(1)}, u32[]{:S(2)}, u32[]{:S(2)}) %collective-permute-start.5) | collective-permute-done | bytes 65568 | tf_op jit(solution)/shard_map/ppermute | solution.py:27
  33.4 0.0 collective-permute-done.6
  33.5 0.0 copy-start
  33.5 0.8 copy-done
  34.2 0.0 all-gather.2.cloned.1.call-update
  34.3 0.0 reduce-scatter.2.cloned.1.call-start
  34.3 10.1 %all-gather.2.cloned.1.call-done = bf16[8,32,2048]{2,1,0:T(8,128)(2,1)} async-done(((bf16[8,32,1024]{2,1,0:T(8,128)(2,1)}), bf16[8,32,2048]{2,1,0:T(8,128)(2,1)}) %all-gather.2.cloned.1.call-update) | async-done | bytes 1048592 | tf_op jit(solution)/shard_map/all_gather | solution.py:72
  44.4 0.0 copy-start.2
  44.5 10.1 %fusion.4 = f32[256,3072]{1,0:T(8,128)} fusion(bf16[256,2048]{1,0:T(8,128)(2,1)} %bitcast.50, bf16[1,2048,3072]{2,1,0:T(8,128)(2,1)} %param.11), kind=kOutput, calls=%fused_computation.7 | convolution fusion | flops 3221225472 | bytes 16777216 | tf_op jit(solution)/shard_map/dot_general | solution.py:33
  54.5 0.0 copy-done.2
  54.5 0.0 copy-start.1
  54.5 17.0 %fusion.12 = bf16[256,2048]{1,0:T(8,128)(2,1)} fusion(bf16[1,3072,2048]{2,1,0:T(8,128)(2,1)} %param.13, bf16[256,2048]{1,0:T(8,128)(2,1)S(1)} %bitcast.51, bf16[1,2048,3072]{2,1,0:T(8,128)(2,1)} %param.12, f32[256,3072]{1,0:T(8,128)} %fusion.4), kind=kOutput, calls=%fused_computation.11 | convolution fusion | flops 6447693824 | bytes 30408704 | tf_op jit(solution)/shard_map/dot_general | solution.py:36
  71.6 0.0 reduce-scatter.2.cloned.1.call-update
  71.6 9.7 %reduce-scatter.2.cloned.1.call-done = bf16[256,1024]{1,0:T(8,128)(2,1)} async-done(((bf16[256,2048]{1,0:T(8,128)(2,1)}), bf16[256,1024]{1,0:T(8,128)(2,1)}) %reduce-scatter.2.cloned.1.call-update) | async-done | bytes 524304 | tf_op jit(solution)/shard_map/reduce_scatter | solution.py:38
  81.3 5.8 %all-to-all-start = ((bf16[8,32,1024]{2,1,0:T(8,128)(2,1)}), bf16[8,32,1024]{2,1,0:T(8,128)(2,1)S(1)}, u32[]{:S(2)}, u32[]{:S(2)}) async-start(bf16[8,32,1024]{2,1,0:T(8,128)(2,1)} %bitcast.49), calls=%async_computation.1 | async-start | bytes 1048576 | tf_op jit(solution)/shard_map/all_to_all | solution.py:76
  87.1 0.0 copy-done.1
  87.1 0.1 copy.13
  87.2 14.9 %all-to-all-done = bf16[8,32,1024]{2,1,0:T(8,128)(2,1)S(1)} async-done(((bf16[8,32,1024]{2,1,0:T(8,128)(2,1)}), bf16[8,32,1024]{2,1,0:T(8,128)(2,1)S(1)}, u32[]{:S(2)}, u32[]{:S(2)}) %all-to-all-start) | async-done | bytes 524320 | tf_op jit(solution)/shard_map/all_to_all | solution.py:76
  102.0 0.9 gather_fusion
  102.9 0.2 reshape.134
  103.1 1.0 multiply_reduce_fusion
  (12 shorter events, 0.1 us)
Async XLA Ops:
  6.5 37.9 %all-gather.2.cloned.1.call-start = ((), (), s32[]{:S(2)}) async-start(), calls=%async_computation.2 | async-start | bytes 1572864 | tf_op jit(solution)/shard_map/all_gather | solution.py:72
  16.3 10.9 %collective-permute-start = (bf16[1,1,32,1024]{3,2,0,1:T(8,128)(2,1)S(1)}, bf16[1,1,32,1024]{3,2,0,1:T(8,128)(2,1)S(1)}, u32[]{:S(2)}, u32[]{:S(2)}) collective-permute-start(bf16[1,1,32,1024]{3,2,0,1:T(8,128)(2,1)S(1)} %get-tuple-element.15), channel_id=1, source_target_pairs={{0,2},{2,4},{4,6},{6,8},{8,10},{10,12},{12,14},{14,0},{1,3},{3,5},... | collective-permute-start | bytes 196616 | tf_op jit(solution)/shard_map/ppermute | solution.py:27
  19.1 9.4 %collective-permute-start.1 = (bf16[1,1,32,1024]{3,2,0,1:T(8,128)(2,1)S(1)}, bf16[1,1,32,1024]{3,2,0,1:T(8,128)(2,1)S(1)}, u32[]{:S(2)}, u32[]{:S(2)}) collective-permute-start(bf16[1,1,32,1024]{3,2,0,1:T(8,128)(2,1)S(1)} %get-tuple-element.14), channel_id=1, source_target_pairs={{0,4},{2,6},{4,8},{6,10},{8,12},{10,14},{12,0},{14,2},{1,5},{3,7},... | collective-permute-start | bytes 196616 | tf_op jit(solution)/shard_map/ppermute | solution.py:27
  20.7 9.8 %collective-permute-start.2 = (bf16[1,1,32,1024]{3,2,0,1:T(8,128)(2,1)S(1)}, bf16[1,1,32,1024]{3,2,0,1:T(8,128)(2,1)S(1)}, u32[]{:S(2)}, u32[]{:S(2)}) collective-permute-start(bf16[1,1,32,1024]{3,2,0,1:T(8,128)(2,1)S(1)} %get-tuple-element.13), channel_id=1, source_target_pairs={{0,6},{2,8},{4,10},{6,12},{8,14},{10,0},{12,2},{14,4},{1,7},{3,9},... | collective-permute-start | bytes 196616 | tf_op jit(solution)/shard_map/ppermute | solution.py:27
  23.3 8.1 %collective-permute-start.3 = (bf16[1,1,32,1024]{3,2,0,1:T(8,128)(2,1)S(1)}, bf16[1,1,32,1024]{3,2,0,1:T(8,128)(2,1)S(1)}, u32[]{:S(2)}, u32[]{:S(2)}) collective-permute-start(bf16[1,1,32,1024]{3,2,0,1:T(8,128)(2,1)S(1)} %get-tuple-element.12), channel_id=1, source_target_pairs={{0,8},{2,10},{4,12},{6,14},{8,0},{10,2},{12,4},{14,6},{1,9},{3,11}... | collective-permute-start | bytes 196616 | tf_op jit(solution)/shard_map/ppermute | solution.py:27
  24.5 7.8 %collective-permute-start.4 = (bf16[1,1,32,1024]{3,2,0,1:T(8,128)(2,1)S(1)}, bf16[1,1,32,1024]{3,2,0,1:T(8,128)(2,1)S(1)}, u32[]{:S(2)}, u32[]{:S(2)}) collective-permute-start(bf16[1,1,32,1024]{3,2,0,1:T(8,128)(2,1)S(1)} %get-tuple-element.11), channel_id=1, source_target_pairs={{0,10},{2,12},{4,14},{6,0},{8,2},{10,4},{12,6},{14,8},{1,11},{3,13... | collective-permute-start | bytes 196616 | tf_op jit(solution)/shard_map/ppermute | solution.py:27
  27.1 6.3 %collective-permute-start.5 = (bf16[1,1,32,1024]{3,2,0,1:T(8,128)(2,1)S(1)}, bf16[1,1,32,1024]{3,2,0,1:T(8,128)(2,1)S(1)}, u32[]{:S(2)}, u32[]{:S(2)}) collective-permute-start(bf16[1,1,32,1024]{3,2,0,1:T(8,128)(2,1)S(1)} %get-tuple-element.10), channel_id=1, source_target_pairs={{0,12},{2,14},{4,0},{6,2},{8,4},{10,6},{12,8},{14,10},{1,13},{3,15... | collective-permute-start | bytes 196616 | tf_op jit(solution)/shard_map/ppermute | solution.py:27
  28.5 4.9 %collective-permute-start.6 = (bf16[1,1,32,1024]{3,2,0,1:T(8,128)(2,1)S(1)}, bf16[1,1,32,1024]{3,2,0,1:T(8,128)(2,1)S(1)}, u32[]{:S(2)}, u32[]{:S(2)}) collective-permute-start(bf16[1,1,32,1024]{3,2,0,1:T(8,128)(2,1)S(1)} %get-tuple-element.9), channel_id=1, source_target_pairs={{0,14},{2,0},{4,2},{6,4},{8,6},{10,8},{12,10},{14,12},{1,15},{3,1}... | collective-permute-start | bytes 196616 | tf_op jit(solution)/shard_map/ppermute | solution.py:27
  33.5 0.8 copy-start
  34.3 47.0 %reduce-scatter.2.cloned.1.call-start = ((), (), s32[]{:S(2)}) async-start(), calls=%async_computation.3 | async-start | bytes 1572864 | tf_op jit(solution)/shard_map/reduce_scatter | solution.py:38
  44.4 10.1 %copy-start.2 = (bf16[8,32,2048]{2,1,0:T(8,128)(2,1)S(1)}, bf16[8,32,2048]{2,1,0:T(8,128)(2,1)}, u32[]{:S(2)}) copy-start(bf16[8,32,2048]{2,1,0:T(8,128)(2,1)} %all-gather.2.cloned.1.call-done) | copy-start | bytes 3145732
  54.5 32.5 %copy-start.1 = (f32[32,4]{0,1:T(4,128)S(1)}, f32[32,4]{0,1:T(4,128)}, u32[]{:S(2)}) copy-start(f32[32,4]{0,1:T(4,128)} %param.10) | copy-start | bytes 1540
  81.3 20.7 %all-to-all-start = ((bf16[8,32,1024]{2,1,0:T(8,128)(2,1)}), bf16[8,32,1024]{2,1,0:T(8,128)(2,1)S(1)}, u32[]{:S(2)}, u32[]{:S(2)}) async-start(bf16[8,32,1024]{2,1,0:T(8,128)(2,1)} %bitcast.49), calls=%async_computation.1 | async-start | bytes 1048576 | tf_op jit(solution)/shard_map/all_to_all | solution.py:76
Sparse Core Ops, SparseCore 0:
  34.4 10.0 all-gather.1
  71.7 9.5 reduce-scatter.1
